TPU v7x, 512 devices: a whole 4x8x8 slice. The times are simulated.
512 devices in a mesh: ep: 128 (over z, y, core), tp: 4 (over x).
Axes of the slice: x: 4, y: 8, z: 8, core: 2. Of those that a mesh axis runs over, the one named last changes fastest.
Arguments:
- tokens: bfloat16 [2048, 1024], P(('ep', 'tp')), may hold values from -6 to 6
- gain_attn: bfloat16 [1024], replicated, may hold values from 0.099609375 to 1.8984375
- gain_ffn: bfloat16 [1024], replicated, may hold values from 0.099609375 to 1.8984375
- w_query: bfloat16 [1024, 512], P(None, 'tp'), may hold values from -0.1875 to 0.1875
- w_key: bfloat16 [1024, 128], replicated, may hold values from -0.1875 to 0.1875
- w_value: bfloat16 [1024, 128], replicated, may hold values from -0.1875 to 0.1875
- w_output: bfloat16 [512, 1024], P('tp'), may hold values from -0.25 to 0.25
- head_bias: float32 [8], replicated, may hold values from -9 to -2
- keys_cache: bfloat16 [2048, 1024, 128], P(('ep', 'tp')), may hold values from -6 to 6
- values_cache: bfloat16 [2048, 1024, 128], P(('ep', 'tp')), may hold values from -6 to 6
- lengths: int32 [2048], P(('ep', 'tp')), may hold values from 256 to 1024
- dense_gate_w: bfloat16 [4096, 1024], P('ep'), may hold values from -0.1875 to 0.1875
- dense_up_w: bfloat16 [4096, 1024], P('ep'), may hold values from -0.1875 to 0.1875
- dense_down_w: bfloat16 [4096, 1024], P('ep'), may hold values from -0.09375 to 0.09375
- mix_gate: bfloat16 [1024], replicated, may hold values from -0.1875 to 0.1875
- expert_gate: bfloat16 [128, 1024, 1024], P('ep', None, 'tp'), may hold values from -0.1875 to 0.1875
- expert_up: bfloat16 [128, 1024, 1024], P('ep', None, 'tp'), may hold values from -0.1875 to 0.1875
- expert_down: bfloat16 [128, 1024, 1024], P('ep', 'tp'), may hold values from -0.09375 to 0.09375
- routes: int32 [2048, 2], P(('ep', 'tp')), may hold values from 0 to 31, all different within a row; in each aligned block of 16 rows (0 to 15, 16 to 31, ...) at most 2 rows name the same one
- route_weights: float32 [2048, 2], P(('ep', 'tp')), may hold values from 0.1 to 0.9
Outputs:
- layer_out: bfloat16 [2048, 1024], P(('ep', 'tp'))
- new_keys: bfloat16 [2048, 128], P(('ep', 'tp'))
- new_values: bfloat16 [2048, 128], P(('ep', 'tp'))
Inputs may be any that keep to these rules, and one draw needn't show every extreme that they name: `routes`: each row names 2 different experts. In each aligned block of 16 rows (the tokens held by one index of ep) no expert is named by more than 2 rows, a bound that some block reaches.
All inputs are finite; a program needn't handle non-finite values.
Results may differ from a plain program's by a relative error of at most 0.01.
Values may be sent and summed in bfloat16 or wider, within the bound.
No kernel may reach another device: no remote copies, remote signals or barrier semaphores. Data moves between devices by JAX's collectives and lax.ppermute only.
A program may use at most 64 MiB of HBM per device.

v0:
```python
import math
import jax
import jax.numpy as jnp
from jax import lax
from jax.sharding import PartitionSpec as P

HEADS = 8
HEAD = 64
TOP = 2
SPLIT = 4
EPS = 1e-06


def laid_out(pieces, dim):
    pieces = jnp.moveaxis(pieces, 0, dim)
    lengths = pieces.shape
    return pieces.reshape(*lengths[:dim], lengths[dim] * lengths[dim + 1], *lengths[dim + 2 :])


def copy_for_each(array, axis):
    copies = jnp.broadcast_to(array, (lax.axis_size(axis), *array.shape))
    return lax.all_to_all(copies, axis, split_axis=0, concat_axis=0, tiled=True)


def collect(array, axis, dim):
    return laid_out(copy_for_each(array, axis), dim)


def split_up(array, dim, size):
    lengths = array.shape
    pieces = array.reshape(*lengths[:dim], size, lengths[dim] // size, *lengths[dim + 1 :])
    return jnp.moveaxis(pieces, dim, 0)


def sent_and_summed(array, axis, dim):
    size = lax.axis_size(axis)
    pieces = lax.all_to_all(split_up(array, dim, size), axis, 0, 0, tiled=True)
    return jnp.sum(pieces.astype(jnp.float32), axis=0)


def partner_2(block, axis, apart):
    count = lax.axis_size(axis)
    route = []
    for low in range(count):
        high = low | 1 << apart
        if high != low and high < count:
            route += [(low, high), (high, low)]
    return lax.ppermute(block, axis, route)


def rms_scale(values, gains):
    widened = values.astype(jnp.float32)
    scaled = widened * lax.rsqrt(jnp.mean(widened * widened, axis=-1, keepdims=True) + EPS)
    return (scaled * gains.astype(jnp.float32)).astype(jnp.bfloat16)


def slot_table(route_ids, experts_total, capacity):
    expert_ids = lax.broadcasted_iota(jnp.int32, route_ids.shape + (experts_total,), route_ids.ndim)
    picked = (route_ids[..., None] == expert_ids).astype(jnp.float32)
    chosen = jnp.sum(picked, axis=-2)
    earlier = jnp.cumsum(chosen, axis=-2) - chosen
    slot_ids = lax.broadcasted_iota(jnp.int32, chosen.shape + (capacity,), chosen.ndim).astype(
        jnp.float32
    )
    table = chosen[..., None] * (earlier[..., None] == slot_ids).astype(jnp.float32)
    return (picked, table)


def stick_read(queries, keys_cache, values_cache, lengths, head_bias):
    seq_count, positions, joined = keys_cache.shape
    kv_heads = joined // HEAD
    groups = HEADS // kv_heads
    query_heads = queries.reshape(seq_count, kv_heads, groups, HEAD)
    key_heads = keys_cache.reshape(seq_count, positions, kv_heads, HEAD)
    value_heads = values_cache.reshape(seq_count, positions, kv_heads, HEAD)
    scores = jnp.einsum(
        "bkgd,bpkd->bkgp", query_heads, key_heads, preferred_element_type=jnp.float32
    )
    scores = scores * (1.0 / math.sqrt(HEAD)) + head_bias.reshape(1, kv_heads, groups, 1)
    position = lax.broadcasted_iota(jnp.int32, scores.shape, 3)
    is_live = position < lengths.reshape(seq_count, 1, 1, 1)
    skipped = jnp.where(is_live, jax.nn.log_sigmoid(-scores), 0.0)
    later_sum = lax.cumsum(skipped, axis=3, reverse=True) - skipped
    weights = jnp.where(is_live, jnp.exp(jax.nn.log_sigmoid(scores) + later_sum), 0.0).astype(
        jnp.bfloat16
    )
    mixed_heads = jnp.einsum(
        "bkgp,bpkd->bkgd", weights, value_heads, preferred_element_type=jnp.float32
    )
    return mixed_heads.astype(jnp.bfloat16).reshape(seq_count, HEADS * HEAD)


def expert_rows(received, gate_local, up_local, down_local):
    dims_in = received.shape
    flat_rows = received.reshape(dims_in[0] * dims_in[1], dims_in[2])
    gate_val = jnp.dot(flat_rows, gate_local, preferred_element_type=jnp.float32)
    up_val = jnp.dot(flat_rows, up_local, preferred_element_type=jnp.float32)
    hidden = (jax.nn.silu(gate_val) * up_val).astype(jnp.bfloat16)
    result = jnp.dot(hidden, down_local, preferred_element_type=jnp.float32)
    return result.reshape(dims_in[0], dims_in[1], down_local.shape[1])


def body(
    tokens,
    gain_attn,
    gain_ffn,
    w_query,
    w_key,
    w_value,
    w_output,
    head_bias,
    keys_cache,
    values_cache,
    lengths,
    dense_gate_w,
    dense_up_w,
    dense_down_w,
    mix_gate,
    expert_gate,
    expert_up,
    expert_down,
    routes,
    route_weights,
):
    own_rows = tokens.shape[0]
    attn_in = rms_scale(tokens, gain_attn)
    query_group = jnp.dot(
        collect(attn_in, "tp", 0), w_query, preferred_element_type=jnp.float32
    ).astype(jnp.bfloat16)
    queries = lax.all_to_all(query_group, "tp", split_axis=0, concat_axis=1, tiled=True)
    new_keys = jnp.dot(attn_in, w_key, preferred_element_type=jnp.float32).astype(jnp.bfloat16)
    new_values = jnp.dot(attn_in, w_value, preferred_element_type=jnp.float32).astype(jnp.bfloat16)
    mixed_heads = stick_read(queries, keys_cache, values_cache, lengths, head_bias)
    heads_group = lax.all_to_all(mixed_heads, "tp", split_axis=1, concat_axis=0, tiled=True)
    attn_sum = sent_and_summed(
        jnp.dot(heads_group, w_output, preferred_element_type=jnp.float32).astype(jnp.bfloat16),
        "tp",
        0,
    )
    residual = (tokens.astype(jnp.float32) + attn_sum).astype(jnp.bfloat16)
    ffn_in = rms_scale(residual, gain_ffn)
    mix_scale = jax.nn.sigmoid(jnp.dot(ffn_in, mix_gate, preferred_element_type=jnp.float32))
    block_rows = lax.all_gather(ffn_in, "ep", axis=0, tiled=True)
    gate_val = jnp.dot(block_rows, dense_gate_w.T, preferred_element_type=jnp.float32)
    up_val = jnp.dot(block_rows, dense_up_w.T, preferred_element_type=jnp.float32)
    hidden_dense = (jax.nn.silu(gate_val) * up_val).astype(jnp.bfloat16)
    down_whole = lax.all_gather(dense_down_w, "ep", axis=0, tiled=True)
    hidden_own = lax.all_to_all(hidden_dense, "ep", split_axis=0, concat_axis=1, tiled=True)
    dense_out = jnp.dot(hidden_own, down_whole, preferred_element_type=jnp.float32)
    group_count = lax.axis_size("ep")
    group_rows = own_rows * lax.axis_size("tp")
    experts_total = group_count // SPLIT
    capacity = max(2, (group_rows * TOP + experts_total - 1) // experts_total)
    group_routes, group_weights = (
        lax.all_gather(routes, "tp", axis=0, tiled=True),
        lax.all_gather(route_weights, "tp", axis=0, tiled=True),
    )
    feature_part = lax.all_to_all(ffn_in, "tp", split_axis=1, concat_axis=0, tiled=True)
    picked, table = slot_table(group_routes, experts_total, capacity)
    weight_of = jnp.sum(group_weights[:, :, None] * picked, axis=1)
    quarter = jnp.einsum(
        "jxc,jd->xcd", table.astype(jnp.bfloat16), feature_part, preferred_element_type=jnp.float32
    ).astype(jnp.bfloat16)
    narrow = quarter.shape[2] // SPLIT
    pieces = (
        quarter.reshape(experts_total, capacity, SPLIT, narrow)
        .transpose(0, 2, 1, 3)
        .reshape(experts_total * SPLIT, capacity, narrow)
    )
    current = lax.all_to_all(pieces, "ep", split_axis=0, concat_axis=0, tiled=True)
    position = lax.axis_index("ep")
    for bit in range(SPLIT.bit_length() - 1):
        partner = partner_2(current, "ep", bit)
        upper = position // (1 << bit) % 2 == 1
        lower_half = jnp.where(upper, partner, current)
        upper_half = jnp.where(upper, current, partner)
        current = jnp.concatenate([lower_half, upper_half], axis=2)
    received = lax.all_gather(current, "tp", axis=2, tiled=True)
    partial_value = expert_rows(received, expert_gate[0], expert_up[0], expert_down[0])
    summed = sent_and_summed(partial_value.astype(jnp.bfloat16), "tp", 2)
    returned = lax.all_to_all(
        summed.astype(jnp.bfloat16), "ep", split_axis=0, concat_axis=0, tiled=True
    ).astype(summed.dtype)
    dims_back = returned.shape
    per_expert = jnp.sum(returned.reshape(experts_total, SPLIT, dims_back[1], dims_back[2]), axis=1)
    combine = table * weight_of[:, :, None]
    moe_group = jnp.einsum("jxc,xcd->jd", combine, per_expert, precision=lax.Precision.HIGHEST)
    moe_out = lax.all_to_all(moe_group, "tp", split_axis=0, concat_axis=1, tiled=True)
    layer_out = (residual.astype(jnp.float32) + moe_out + mix_scale[:, None] * dense_out).astype(
        jnp.bfloat16
    )
    return (layer_out, new_keys, new_values)


def solution(mesh):
    return jax.shard_map(
        body,
        mesh=mesh,
        in_specs=(
            P(("ep", "tp"), None),
            P(),
            P(),
            P(None, "tp"),
            P(),
            P(),
            P("tp", None),
            P(),
            P(("ep", "tp"), None, None),
            P(("ep", "tp"), None, None),
            P(("ep", "tp")),
            P("ep", None),
            P("ep", None),
            P("ep", None),
            P(),
            P("ep", None, "tp"),
            P("ep", None, "tp"),
            P("ep", "tp", None),
            P(("ep", "tp"), None),
            P(("ep", "tp"), None),
        ),
        out_specs=(P(("ep", "tp"), None), P(("ep", "tp"), None), P(("ep", "tp"), None)),
        check_vma=False,
    )
```

profile of v0, /device:TPU:1, one launch (start us, length us, event | category | flops | bytes accessed | tf_op | source)
XLA Modules:
  0.0 277.3 jit_solution(14062329265283297305)
XLA Ops:
  9.6 8.9 %all_to_all.114 = bf16[4,4,1024]{2,1,0:T(4,128)(2,1)S(1)} all-to-all(bf16[4,4,1024]{2,1,0:T(4,128)(2,1)S(1)} %broadcast_in_dim.5), channel_id=1, replica_groups=mesh['ep'=128,'tp'=4] {'tp'}, dimensions={0} | all-to-all | bytes 65536 | tf_op jit(solution)/shard_map/all_to_all | solution.py:22
  18.6 1.7 convolution_convert_fusion.4
  20.3 3.2 %all-to-all-start.1 = ((bf16[4,4,128]{2,1,0:T(4,128)(2,1)}), bf16[4,4,128]{2,1,0:T(4,128)(2,1)S(1)}, u32[]{:S(2)}, u32[]{:S(2)}) async-start(bf16[4,4,128]{2,1,0:T(4,128)(2,1)} %bitcast), calls=%async_computation.1 | async-start | bytes 8192 | tf_op jit(solution)/shard_map/all_to_all | solution.py:130
  23.5 1.5 copy.94
  26.3 1.5 copy.95
  28.5 1.6 fusion.19
  30.2 39.6 %reduce-window.6 = f32[4,2,4,8,128]{4,3,2,1,0:T(8,128)S(1)} reduce-window(f32[4,2,4,8,128]{4,3,2,1,0:T(8,128)S(1)} %reshape.112, f32[]{:T(128)} %constant.60.clone.1), window={size=1x1x1x1x128 pad=0_0x0_0x0_0x0_0x0_127}, to_apply=%region_1.2 | reduce-window | flops 4161536 | bytes 262148 | tf_op jit(solution)/shard_map/reduce-window
  70.0 1.4 reduce-window.9
  71.6 1.5 convolution_convert_fusion.3
  73.2 8.1 %all_to_all.115 = bf16[4,4,128]{2,0,1:T(4,128)(2,1)S(1)} all-to-all(bf16[4,4,128]{2,0,1:T(4,128)(2,1)S(1)} %copy.96), channel_id=1, replica_groups=mesh['ep'=128,'tp'=4] {'tp'}, dimensions={1} | all-to-all | bytes 8192 | tf_op jit(solution)/shard_map/all_to_all | solution.py:134
  82.1 3.3 %all-to-all-start.3 = ((bf16[4,4,1024]{2,1,0:T(4,128)(2,1)}), bf16[4,4,1024]{2,1,0:T(4,128)(2,1)S(1)}, u32[]{:S(2)}, u32[]{:S(2)}) async-start(bf16[4,4,1024]{2,1,0:T(4,128)(2,1)} %reshape.115), calls=%async_computation.3 | async-start | bytes 65536 | tf_op jit(solution)/shard_map/all_to_all | solution.py:37
  86.1 3.5 %all-to-all-done.3 = bf16[4,4,1024]{2,1,0:T(4,128)(2,1)S(1)} async-done(((bf16[4,4,1024]{2,1,0:T(4,128)(2,1)}), bf16[4,4,1024]{2,1,0:T(4,128)(2,1)S(1)}, u32[]{:S(2)}, u32[]{:S(2)}) %all-to-all-start.3) | async-done | bytes 32800 | tf_op jit(solution)/shard_map/all_to_all | solution.py:37
  91.3 6.5 %all-gather = s32[4,4,2]{1,2,0:T(2,128)S(1)} all-gather(s32[1,4,2]{1,2,0:T(2,128)} %bitcast.110), channel_id=1, replica_groups=mesh['ep'=128,'tp'=4] {'tp'}, dimensions={0}, use_global_device_ids=true | all-gather | bytes 160 | tf_op jit(solution)/shard_map/all_gather | solution.py:155
  97.8 6.4 %all-gather.1 = f32[4,4,2]{1,2,0:T(2,128)S(1)} all-gather(f32[1,4,2]{1,2,0:T(2,128)} %bitcast.111), channel_id=1, replica_groups=mesh['ep'=128,'tp'=4] {'tp'}, dimensions={0}, use_global_device_ids=true | all-gather | bytes 160 | tf_op jit(solution)/shard_map/all_gather | solution.py:156
  105.1 3.2 %all-to-all-start.4 = ((bf16[4,4,256]{2,0,1:T(4,128)(2,1)}), bf16[4,4,256]{2,0,1:T(4,128)(2,1)S(1)}, u32[]{:S(2)}, u32[]{:S(2)}) async-start(bf16[4,4,256]{2,0,1:T(4,128)(2,1)} %bitcast.11), calls=%async_computation.4 | async-start | bytes 16384 | tf_op jit(solution)/shard_map/all_to_all | solution.py:158
  108.4 4.1 %all-to-all-done.4 = bf16[4,4,256]{2,0,1:T(4,128)(2,1)S(1)} async-done(((bf16[4,4,256]{2,0,1:T(4,128)(2,1)}), bf16[4,4,256]{2,0,1:T(4,128)(2,1)S(1)}, u32[]{:S(2)}, u32[]{:S(2)}) %all-to-all-start.4) | async-done | bytes 8224 | tf_op jit(solution)/shard_map/all_to_all | solution.py:158
  112.9 37.9 %all_to_all.116 = bf16[128,2,64]{2,1,0:T(2,128)(2,1)S(1)} all-to-all(bf16[128,2,64]{2,1,0:T(2,128)(2,1)S(1)} %bitcast.101), channel_id=1, replica_groups=mesh['ep'=128,'tp'=4] {'ep'}, dimensions={0} | all-to-all | bytes 65536 | tf_op jit(solution)/shard_map/all_to_all | solution.py:170
  150.8 2.5 collective-permute-start
  154.4 2.4 collective-permute-start.1
  156.9 2.5 collective-permute-done.1
  159.8 9.9 %all_gather.17 = bf16[128,2,1024]{2,1,0:T(2,128)(2,1)S(1)} all-gather(bf16[128,2,256]{2,1,0:T(2,128)(2,1)S(1)} %pad_maximum_fusion), channel_id=1, replica_groups=mesh['ep'=128,'tp'=4] {'tp'}, dimensions={2}, use_global_device_ids=true | all-gather | bytes 655360 | tf_op jit(solution)/shard_map/all_gather | solution.py:178
  170.3 1.3 fusion
  172.0 9.3 %all_to_all.117 = bf16[4,128,2,256]{3,1,2,0:T(8,128)(2,1)S(1)} all-to-all(bf16[4,128,2,256]{3,1,2,0:T(8,128)(2,1)S(1)} %bitcast.91), channel_id=1, replica_groups=mesh['ep'=128,'tp'=4] {'tp'}, dimensions={0} | all-to-all | bytes 1048576 | tf_op jit(solution)/shard_map/all_to_all | solution.py:37
  182.2 9.0 %all-to-all-start.7 = ((bf16[128,2,256]{2,1,0:T(2,128)(2,1)}), bf16[128,2,256]{2,1,0:T(2,128)(2,1)S(1)}, u32[]{:S(2)}, u32[]{:S(2)}) async-start(bf16[128,2,256]{2,1,0:T(2,128)(2,1)} %copy.104), calls=%async_computation.7 | async-start | bytes 262144 | tf_op jit(solution)/shard_map/all_to_all | solution.py:181
  192.8 11.7 %all-to-all-done.7 = bf16[128,2,256]{2,1,0:T(2,128)(2,1)S(1)} async-done(((bf16[128,2,256]{2,1,0:T(2,128)(2,1)}), bf16[128,2,256]{2,1,0:T(2,128)(2,1)S(1)}, u32[]{:S(2)}, u32[]{:S(2)}) %all-to-all-start.7) | async-done | bytes 131104 | tf_op jit(solution)/shard_map/all_to_all | solution.py:181
  204.6 1.4 reshape.128
  207.6 5.7 %all-to-all-start.9 = ((bf16[128,4,32]{2,1,0:T(4,128)(2,1)}), bf16[128,4,32]{2,1,0:T(4,128)(2,1)S(1)}, u32[]{:S(2)}, u32[]{:S(2)}) async-start(bf16[128,4,32]{2,1,0:T(4,128)(2,1)} %bitcast.27), calls=%async_computation.9 | async-start | bytes 262144 | tf_op jit(solution)/shard_map/all_to_all | solution.py:148
  214.2 12.0 %all-to-all-done.9 = bf16[128,4,32]{2,1,0:T(4,128)(2,1)S(1)} async-done(((bf16[128,4,32]{2,1,0:T(4,128)(2,1)}), bf16[128,4,32]{2,1,0:T(4,128)(2,1)S(1)}, u32[]{:S(2)}, u32[]{:S(2)}) %all-to-all-start.9) | async-done | bytes 32800 | tf_op jit(solution)/shard_map/all_to_all | solution.py:148
  226.2 3.2 %all-to-all-start.8 = ((f32[4,4,256]{2,1,0:T(4,128)}), f32[4,4,256]{2,1,0:T(4,128)S(1)}, u32[]{:S(2)}, u32[]{:S(2)}) async-start(f32[4,4,256]{2,1,0:T(4,128)} %convolution_bitcast_fusion), calls=%async_computation.8 | async-start | bytes 32768 | tf_op jit(solution)/shard_map/all_to_all | solution.py:188
  230.5 3.1 %all-to-all-done.8 = f32[4,4,256]{2,1,0:T(4,128)S(1)} async-done(((f32[4,4,256]{2,1,0:T(4,128)}), f32[4,4,256]{2,1,0:T(4,128)S(1)}, u32[]{:S(2)}, u32[]{:S(2)}) %all-to-all-start.8) | async-done | bytes 16416 | tf_op jit(solution)/shard_map/all_to_all | solution.py:188
  233.7 31.7 %all-gather.6.cloned.1.call-done = bf16[4096,1024]{1,0:T(8,128)(2,1)} async-done(((bf16[32,1024]{1,0:T(8,128)(2,1)}), bf16[4096,1024]{1,0:T(8,128)(2,1)}) %all-gather.6.cloned.1.call-update) | async-done | bytes 8388624 | tf_op jit(solution)/shard_map/all_gather | solution.py:147
  265.3 5.2 %fusion.4 = bf16[4,1024]{1,0:T(4,128)(2,1)} fusion(bf16[4,4096]{1,0:T(4,128)(2,1)S(1)} %all_to_all.103, bf16[4096,1024]{1,0:T(8,128)(2,1)} %all-gather.6.cloned.1.call-done, f32[4,1024]{1,0:T(4,128)S(1)} %bitcast.105, bf16[4,1024]{1,0:T(4,128)(2,1)S(1)} %get-tuple-element.6, f32[4]{0:T(128)S(1)} %fusion.8), kind=kOutput, calls=%fused_computation.12 | convolution fusion | flops 33574912 | bytes 8454160 | tf_op jit(solution)/shard_map/dot_general | solution.py:149
  (85 shorter events, 17.8 us)
Async XLA Ops:
  7.2 164.5 %copy-start = (bf16[1,256,1024]{2,1,0:T(8,128)(2,1)S(1)}, bf16[1,256,1024]{2,1,0:T(8,128)(2,1)}, u32[]{:S(2)}) copy-start(bf16[1,256,1024]{2,1,0:T(8,128)(2,1)} %param.37) | copy-start | bytes 1572868
  7.2 82.5 %copy-start.5 = (bf16[4,1024]{1,0:T(4,128)(2,1)S(1)}, bf16[4,1024]{1,0:T(4,128)(2,1)}, u32[]{:S(2)}) copy-start(bf16[4,1024]{1,0:T(4,128)(2,1)} %param.20) | copy-start | bytes 24580
  7.2 74.2 %copy-start.2 = (bf16[128,1024]{1,0:T(8,128)(2,1)S(1)}, bf16[128,1024]{1,0:T(8,128)(2,1)}, u32[]{:S(2)}) copy-start(bf16[128,1024]{1,0:T(8,128)(2,1)} %param.26) | copy-start | bytes 786436
  7.2 162.7 %copy-start.1 = (bf16[1,1024,256]{2,1,0:T(8,128)(2,1)S(1)}, bf16[1,1024,256]{2,1,0:T(8,128)(2,1)}, u32[]{:S(2)}) copy-start(bf16[1,1024,256]{2,1,0:T(8,128)(2,1)} %param.35) | copy-start | bytes 1572868
  20.3 7.5 %all-to-all-start.1 = ((bf16[4,4,128]{2,1,0:T(4,128)(2,1)}), bf16[4,4,128]{2,1,0:T(4,128)(2,1)S(1)}, u32[]{:S(2)}, u32[]{:S(2)}) async-start(bf16[4,4,128]{2,1,0:T(4,128)(2,1)} %bitcast), calls=%async_computation.1 | async-start | bytes 8192 | tf_op jit(solution)/shard_map/all_to_all | solution.py:130
  30.1 161.1 %copy-start.3 = (bf16[1024,128]{1,0:T(8,128)(2,1)S(1)}, bf16[1024,128]{1,0:T(8,128)(2,1)}, u32[]{:S(2)}) copy-start(bf16[1024,128]{1,0:T(8,128)(2,1)} %param.25) | copy-start | bytes 786436
  30.1 161.9 %copy-start.8 = (bf16[1024]{0:T(1024)(128)(2,1)S(1)}, bf16[1024]{0:T(1024)(128)(2,1)}, u32[]{:S(2)}) copy-start(bf16[1024]{0:T(1024)(128)(2,1)} %param.34) | copy-start | bytes 6148
  30.2 161.9 %copy-start.4 = (bf16[1024,128]{1,0:T(8,128)(2,1)S(1)}, bf16[1024,128]{1,0:T(8,128)(2,1)}, u32[]{:S(2)}) copy-start(bf16[1024,128]{1,0:T(8,128)(2,1)} %param.24) | copy-start | bytes 786436
  71.6 134.4 %copy-start.6 = (bf16[32,1024]{1,0:T(8,128)(2,1)S(1)}, bf16[32,1024]{1,0:T(8,128)(2,1)}, u32[]{:S(2)}) copy-start(bf16[32,1024]{1,0:T(8,128)(2,1)} %param.31) | copy-start | bytes 196612
  73.1 133.3 %copy-start.7 = (bf16[32,1024]{1,0:T(8,128)(2,1)S(1)}, bf16[32,1024]{1,0:T(8,128)(2,1)}, u32[]{:S(2)}) copy-start(bf16[32,1024]{1,0:T(8,128)(2,1)} %param.32) | copy-start | bytes 196612
  82.1 7.5 %all-to-all-start.3 = ((bf16[4,4,1024]{2,1,0:T(4,128)(2,1)}), bf16[4,4,1024]{2,1,0:T(4,128)(2,1)S(1)}, u32[]{:S(2)}, u32[]{:S(2)}) async-start(bf16[4,4,1024]{2,1,0:T(4,128)(2,1)} %reshape.115), calls=%async_computation.3 | async-start | bytes 65536 | tf_op jit(solution)/shard_map/all_to_all | solution.py:37
  85.4 119.2 %all-gather.8.cloned.1.call-start = ((), (), s32[]{:S(2)}) async-start(), calls=%async_computation.11 | async-start | bytes 1056768 | tf_op jit(solution)/shard_map/all_gather | solution.py:143
  90.5 174.8 %all-gather.6.cloned.1.call-start = ((), (), s32[]{:S(2)}) async-start(), calls=%async_computation.10 | async-start | bytes 8454144 | tf_op jit(solution)/shard_map/all_gather | solution.py:147
  105.1 7.4 %all-to-all-start.4 = ((bf16[4,4,256]{2,0,1:T(4,128)(2,1)}), bf16[4,4,256]{2,0,1:T(4,128)(2,1)S(1)}, u32[]{:S(2)}, u32[]{:S(2)}) async-start(bf16[4,4,256]{2,0,1:T(4,128)(2,1)} %bitcast.11), calls=%async_computation.4 | async-start | bytes 16384 | tf_op jit(solution)/shard_map/all_to_all | solution.py:158
  150.8 3.3 %collective-permute-start = (bf16[128,2,64]{2,1,0:T(2,128)(2,1)S(1)}, bf16[128,2,64]{2,1,0:T(2,128)(2,1)S(1)}, u32[]{:S(2)}, u32[]{:S(2)}) collective-permute-start(bf16[128,2,64]{2,1,0:T(2,128)(2,1)S(1)} %all_to_all.116), channel_id=1, source_target_pairs={{0,4},{4,0},{8,12},{12,8},{16,20},{20,16},{24,28},{28,24},{32,36},... | collective-permute-start | bytes 98312 | tf_op jit(solution)/shard_map/ppermute | solution.py:48
  154.4 5.0 %collective-permute-start.1 = (bf16[128,2,128]{2,1,0:T(2,128)(2,1)S(1)}, bf16[128,2,128]{2,1,0:T(2,128)(2,1)S(1)}, u32[]{:S(2)}, u32[]{:S(2)}) collective-permute-start(bf16[128,2,128]{2,1,0:T(2,128)(2,1)S(1)} %pad_maximum_fusion.2), channel_id=1, source_target_pairs={{0,8},{8,0},{4,12},{12,4},{16,24},{24,16},{20,28},{28,20},{32,40},... | collective-permute-start | bytes 196616 | tf_op jit(solution)/shard_map/ppermute | solution.py:48
  182.2 22.2 %all-to-all-start.7 = ((bf16[128,2,256]{2,1,0:T(2,128)(2,1)}), bf16[128,2,256]{2,1,0:T(2,128)(2,1)S(1)}, u32[]{:S(2)}, u32[]{:S(2)}) async-start(bf16[128,2,256]{2,1,0:T(2,128)(2,1)} %copy.104), calls=%async_computation.7 | async-start | bytes 262144 | tf_op jit(solution)/shard_map/all_to_all | solution.py:181
  207.6 18.6 %all-to-all-start.9 = ((bf16[128,4,32]{2,1,0:T(4,128)(2,1)}), bf16[128,4,32]{2,1,0:T(4,128)(2,1)S(1)}, u32[]{:S(2)}, u32[]{:S(2)}) async-start(bf16[128,4,32]{2,1,0:T(4,128)(2,1)} %bitcast.27), calls=%async_computation.9 | async-start | bytes 262144 | tf_op jit(solution)/shard_map/all_to_all | solution.py:148
  226.2 7.4 %all-to-all-start.8 = ((f32[4,4,256]{2,1,0:T(4,128)}), f32[4,4,256]{2,1,0:T(4,128)S(1)}, u32[]{:S(2)}, u32[]{:S(2)}) async-start(f32[4,4,256]{2,1,0:T(4,128)} %convolution_bitcast_fusion), calls=%async_computation.8 | async-start | bytes 32768 | tf_op jit(solution)/shard_map/all_to_all | solution.py:188
Sparse Core Ops, SparseCore 0:
  90.7 86.9 all-gather.7
  180.8 84.4 all-gather.5
where the time goes:
time: 278 us; the launch traced here: 277 us
  blocking collectives  87.1 us (31%)
  waiting for transfers between devices  70.3 us (25%)
  other arithmetic  46.7 us (17%)
  starting transfers between devices  32.7 us (12%)
  matrix products  16.3 us (6%)
  between operations  14.4 us (5%)
  local copies, waits for them, and re-layouts  9.8 us (4%)
    another operation x2, other arithmetic  41.1 us
    all_to_all x1, blocking collectives, body(): lax.all_to_all(pieces, 'ep', split_axis=0, concat_axis=0, tiled=True)  37.9 us
    all_gather x1, waiting for transfers between devices, body(): down_whole = lax.all_gather(dense_down_w, 'ep', axis=0, tiled=True)  31.7 us
    all_to_all x1, waiting for transfers between devices, body(): lax.all_to_all(hidden_dense, 'ep', split_axis=0, concat_axis=1, tiled=True)  12 us
    all_to_all x1, waiting for transfers between devices, body(): lax.all_to_all(summed.astype(jnp.bfloat16), 'ep', split_axis=0, concat_ax...  11.7 us
    all_gather x1, blocking collectives, body(): received = lax.all_gather(current, 'tp', axis=2, tiled=True)  9.95 us
    all_to_all x1, blocking collectives, sent_and_summed(): pieces = lax.all_to_all(split_up(array, dim, size), axis, 0, 0, tiled=True)  9.33 us
    all_to_all x1, starting transfers between devices, body(): lax.all_to_all(summed.astype(jnp.bfloat16), 'ep', split_axis=0, concat_ax...  9.04 us
  transfers between devices with their start and end apart: 10, of which 8 were waited for; matrix products, arithmetic and copies ran while one was open for 6% of the time, Pallas kernels for 0%

commit v1 on v0

--- a/solution.py
+++ b/solution.py
@@ -144,7 +144,9 @@
     gate_val = jnp.dot(block_rows, dense_gate_w.T, preferred_element_type=jnp.float32)
     up_val = jnp.dot(block_rows, dense_up_w.T, preferred_element_type=jnp.float32)
     hidden_dense = (jax.nn.silu(gate_val) * up_val).astype(jnp.bfloat16)
-    down_whole = lax.all_gather(dense_down_w, "ep", axis=0, tiled=True)
+    down_whole = jnp.concatenate(
+        lax.all_to_all(jnp.stack([dense_down_w] * lax.axis_size("ep")), "ep", 0, 0), axis=0
+    )
     hidden_own = lax.all_to_all(hidden_dense, "ep", split_axis=0, concat_axis=1, tiled=True)
     dense_out = jnp.dot(hidden_own, down_whole, preferred_element_type=jnp.float32)
     group_count = lax.axis_size("ep")

time: 278 us -> 526 us (1.89)
  the two profiles are of different devices: /device:TPU:1 before, /device:TPU:17 now
where the time goes in v1:
time: 526 us; the launch traced here: 525 us
  waiting for transfers between devices  296 us (56%)
  blocking collectives  96.1 us (18%)
  other arithmetic  46.7 us (9%)
  starting transfers between devices  41.9 us (8%)
  matrix products  15.4 us (3%)
  between operations  14.5 us (3%)
  local copies, waits for them, and re-layouts  13.8 us (3%)
    all_to_all x1, waiting for transfers between devices, body(): lax.all_to_all(jnp.stack([dense_down_w] * lax.axis_size('ep')), 'ep', 0, 0)  253 us
    another operation x2, other arithmetic  41.1 us
    all_to_all x1, blocking collectives, body(): lax.all_to_all(pieces, 'ep', split_axis=0, concat_axis=0, tiled=True)  35.5 us
    all_gather x1, waiting for transfers between devices, body(): block_rows = lax.all_gather(ffn_in, 'ep', axis=0, tiled=True)  21.8 us
    all_to_all x1, blocking collectives, body(): lax.all_to_all(hidden_dense, 'ep', split_axis=0, concat_axis=1, tiled=True)  20.4 us
    all_to_all x1, starting transfers between devices, body(): lax.all_to_all(summed.astype(jnp.bfloat16), 'ep', split_axis=0, concat_ax...  11.3 us
    all_to_all x1, waiting for transfers between devices, body(): lax.all_to_all(summed.astype(jnp.bfloat16), 'ep', split_axis=0, concat_ax...  10.9 us
  transfers between devices with their start and end apart: 10, of which 7 were waited for; matrix products, arithmetic and copies ran while one was open for 3% of the time, Pallas kernels for 0%

profile of v1, /device:TPU:17, one launch (start us, length us, event | category | flops | bytes accessed | tf_op | source)
XLA Modules:
  0.0 524.5 jit_solution(2146650487934912620)
XLA Ops:
  9.6 8.1 %all_to_all.116 = bf16[4,4,1024]{2,1,0:T(4,128)(2,1)S(1)} all-to-all(bf16[4,4,1024]{2,1,0:T(4,128)(2,1)S(1)} %broadcast_in_dim.5), channel_id=1, replica_groups=mesh['ep'=128,'tp'=4] {'tp'}, dimensions={0} | all-to-all | bytes 65536 | tf_op jit(solution)/shard_map/all_to_all | solution.py:22
  17.7 1.7 convolution_convert_fusion.4
  19.4 3.2 all-to-all-start.1
  22.7 1.5 copy.96
  25.5 1.5 copy.95
  27.7 1.6 fusion.20
  29.4 39.6 %reduce-window.6 = f32[4,2,4,8,128]{4,3,2,1,0:T(8,128)S(1)} reduce-window(f32[4,2,4,8,128]{4,3,2,1,0:T(8,128)S(1)} %reshape.115, f32[]{:T(128)} %constant.60.clone.1), window={size=1x1x1x1x128 pad=0_0x0_0x0_0x0_0x0_127}, to_apply=%region_1.2 | reduce-window | flops 4161536 | bytes 262148 | tf_op jit(solution)/shard_map/reduce-window
  69.1 1.4 reduce-window.9
  70.8 1.5 convolution_convert_fusion.3
  73.0 4.2 all-to-all-start.2
  77.2 8.1 %all-gather.1 = f32[4,4,2]{1,2,0:T(2,128)S(1)} all-gather(f32[1,4,2]{1,2,0:T(2,128)} %bitcast.119), channel_id=1, replica_groups=mesh['ep'=128,'tp'=4] {'tp'}, dimensions={0}, use_global_device_ids=true | all-gather | bytes 160 | tf_op jit(solution)/shard_map/all_gather | solution.py:158
  85.3 5.6 %all-gather = s32[4,4,2]{1,2,0:T(2,128)S(1)} all-gather(s32[1,4,2]{1,2,0:T(2,128)} %bitcast.120), channel_id=1, replica_groups=mesh['ep'=128,'tp'=4] {'tp'}, dimensions={0}, use_global_device_ids=true | all-gather | bytes 160 | tf_op jit(solution)/shard_map/all_gather | solution.py:157
  91.8 3.3 all-to-all-start.3
  95.9 3.5 all-to-all-done.3
  100.2 3.2 all-to-all-start.4
  103.6 4.0 all-to-all-done.4
  108.0 35.5 %all_to_all.117 = bf16[128,2,64]{2,1,0:T(2,128)(2,1)S(1)} all-to-all(bf16[128,2,64]{2,1,0:T(2,128)(2,1)S(1)} %bitcast.110), channel_id=1, replica_groups=mesh['ep'=128,'tp'=4] {'ep'}, dimensions={0} | all-to-all | bytes 65536 | tf_op jit(solution)/shard_map/all_to_all | solution.py:172
  143.5 2.5 collective-permute-start
  147.1 2.3 collective-permute-start.1
  150.2 2.0 collective-permute-done.1
  152.5 9.0 %all_gather.14 = bf16[128,2,1024]{2,1,0:T(2,128)(2,1)S(1)} all-gather(bf16[128,2,256]{2,1,0:T(2,128)(2,1)S(1)} %pad_maximum_fusion), channel_id=1, replica_groups=mesh['ep'=128,'tp'=4] {'tp'}, dimensions={2}, use_global_device_ids=true | all-gather | bytes 655360 | tf_op jit(solution)/shard_map/all_gather | solution.py:180
  162.9 9.3 %all_to_all.118 = bf16[4,128,2,256]{3,1,2,0:T(8,128)(2,1)S(1)} all-to-all(bf16[4,128,2,256]{3,1,2,0:T(8,128)(2,1)S(1)} %bitcast.100), channel_id=1, replica_groups=mesh['ep'=128,'tp'=4] {'tp'}, dimensions={0} | all-to-all | bytes 1048576 | tf_op jit(solution)/shard_map/all_to_all | solution.py:37
  173.1 11.3 %all-to-all-start.7 = ((bf16[128,2,256]{2,1,0:T(2,128)(2,1)}), bf16[128,2,256]{2,1,0:T(2,128)(2,1)S(1)}, u32[]{:S(2)}, u32[]{:S(2)}) async-start(bf16[128,2,256]{2,1,0:T(2,128)(2,1)} %copy.105), calls=%async_computation.7 | async-start | bytes 262144 | tf_op jit(solution)/shard_map/all_to_all | solution.py:183
  184.4 10.9 %all-to-all-done.7 = bf16[128,2,256]{2,1,0:T(2,128)(2,1)S(1)} async-done(((bf16[128,2,256]{2,1,0:T(2,128)(2,1)}), bf16[128,2,256]{2,1,0:T(2,128)(2,1)S(1)}, u32[]{:S(2)}, u32[]{:S(2)}) %all-to-all-start.7) | async-done | bytes 131104 | tf_op jit(solution)/shard_map/all_to_all | solution.py:183
  196.3 3.2 all-to-all-start.8
  199.6 21.8 %all-gather.5.cloned.1.call-done = bf16[128,4,1024]{2,1,0:T(4,128)(2,1)} async-done(((bf16[1,4,1024]{2,1,0:T(4,128)(2,1)}), bf16[128,4,1024]{2,1,0:T(4,128)(2,1)}) %all-gather.5.cloned.1.call-update) | async-done | bytes 1048592 | tf_op jit(solution)/shard_map/all_gather | solution.py:143
  221.3 1.3 reshape.131
  223.7 20.4 %all_to_all.119 = bf16[128,4,32]{2,1,0:T(4,128)(2,1)S(1)} all-to-all(bf16[128,4,32]{2,1,0:T(4,128)(2,1)S(1)} %bitcast.107), channel_id=1, replica_groups=mesh['ep'=128,'tp'=4] {'ep'}, dimensions={0} | all-to-all | bytes 65536 | tf_op jit(solution)/shard_map/all_to_all | solution.py:150
  244.1 4.3 stack.2
  248.4 8.6 %all-to-all-start.10 = ((bf16[128,32,1024]{2,1,0:T(8,128)(2,1)}), bf16[128,32,1024]{2,1,0:T(8,128)(2,1)}, u32[]{:S(2)}, u32[]{:S(2)}) async-start(bf16[128,32,1024]{2,1,0:T(8,128)(2,1)} %stack.2), calls=%async_computation.10 | async-start | bytes 16777216 | tf_op jit(solution)/shard_map/all_to_all | solution.py:148
  259.3 253.2 %all-to-all-done.10 = bf16[128,32,1024]{2,1,0:T(8,128)(2,1)} async-done(((bf16[128,32,1024]{2,1,0:T(8,128)(2,1)}), bf16[128,32,1024]{2,1,0:T(8,128)(2,1)}, u32[]{:S(2)}, u32[]{:S(2)}) %all-to-all-start.10) | async-done | bytes 8388640 | tf_op jit(solution)/shard_map/all_to_all | solution.py:148
  512.4 5.3 %fusion.5 = bf16[4,1024]{1,0:T(4,128)(2,1)} fusion(bf16[128,32,1024]{2,1,0:T(8,128)(2,1)} %all-to-all-done.10, bf16[128,4,32]{2,1,0:T(4,128)(2,1)S(1)} %all_to_all.119, f32[4,1024]{1,0:T(4,128)S(1)} %bitcast.113, bf16[4,1024]{1,0:T(4,128)(2,1)S(1)} %get-tuple-element.6, f32[4]{0:T(128)S(1)} %fusion.9), kind=kOutput, calls=%fused_computation.13 | convolution fusion | flops 33574912 | bytes 8454160 | tf_op jit(solution)/shard_map/dot_general | solution.py:151
  (87 shorter events, 17.0 us)
Async XLA Ops:
  7.2 155.3 %copy-start = (bf16[1,256,1024]{2,1,0:T(8,128)(2,1)S(1)}, bf16[1,256,1024]{2,1,0:T(8,128)(2,1)}, u32[]{:S(2)}) copy-start(bf16[1,256,1024]{2,1,0:T(8,128)(2,1)} %param.37) | copy-start | bytes 1572868
  7.2 92.2 %copy-start.5 = (bf16[4,1024]{1,0:T(4,128)(2,1)S(1)}, bf16[4,1024]{1,0:T(4,128)(2,1)}, u32[]{:S(2)}) copy-start(bf16[4,1024]{1,0:T(4,128)(2,1)} %param.20) | copy-start | bytes 24580
  7.2 83.9 %copy-start.2 = (bf16[128,1024]{1,0:T(8,128)(2,1)S(1)}, bf16[128,1024]{1,0:T(8,128)(2,1)}, u32[]{:S(2)}) copy-start(bf16[128,1024]{1,0:T(8,128)(2,1)} %param.26) | copy-start | bytes 786436
  7.2 154.6 %copy-start.1 = (bf16[1,1024,256]{2,1,0:T(8,128)(2,1)S(1)}, bf16[1,1024,256]{2,1,0:T(8,128)(2,1)}, u32[]{:S(2)}) copy-start(bf16[1,1024,256]{2,1,0:T(8,128)(2,1)} %param.35) | copy-start | bytes 1572868
  19.4 7.5 %all-to-all-start.1 = ((bf16[4,4,128]{2,1,0:T(4,128)(2,1)}), bf16[4,4,128]{2,1,0:T(4,128)(2,1)S(1)}, u32[]{:S(2)}, u32[]{:S(2)}) async-start(bf16[4,4,128]{2,1,0:T(4,128)(2,1)} %bitcast), calls=%async_computation.1 | async-start | bytes 8192 | tf_op jit(solution)/shard_map/all_to_all | solution.py:130
  29.3 132.8 %copy-start.10 = (bf16[1,1024,256]{2,1,0:T(8,128)(2,1)S(1)}, bf16[1,1024,256]{2,1,0:T(8,128)(2,1)}, u32[]{:S(2)}) copy-start(bf16[1,1024,256]{2,1,0:T(8,128)(2,1)} %param.36) | copy-start | bytes 1572868
  70.8 151.8 %copy-start.7 = (bf16[32,1024]{1,0:T(8,128)(2,1)S(1)}, bf16[32,1024]{1,0:T(8,128)(2,1)}, u32[]{:S(2)}) copy-start(bf16[32,1024]{1,0:T(8,128)(2,1)} %param.31) | copy-start | bytes 196612
  72.3 150.8 %copy-start.8 = (bf16[32,1024]{1,0:T(8,128)(2,1)S(1)}, bf16[32,1024]{1,0:T(8,128)(2,1)}, u32[]{:S(2)}) copy-start(bf16[32,1024]{1,0:T(8,128)(2,1)} %param.32) | copy-start | bytes 196612
  73.0 18.1 %all-to-all-start.2 = ((bf16[4,4,128]{2,0,1:T(4,128)(2,1)}), bf16[4,4,128]{2,0,1:T(4,128)(2,1)S(1)}, u32[]{:S(2)}, u32[]{:S(2)}) async-start(bf16[4,4,128]{2,0,1:T(4,128)(2,1)} %copy.97), calls=%async_computation.2 | async-start | bytes 8192 | tf_op jit(solution)/shard_map/all_to_all | solution.py:134
  91.8 7.5 %all-to-all-start.3 = ((bf16[4,4,1024]{2,1,0:T(4,128)(2,1)}), bf16[4,4,1024]{2,1,0:T(4,128)(2,1)S(1)}, u32[]{:S(2)}, u32[]{:S(2)}) async-start(bf16[4,4,1024]{2,1,0:T(4,128)(2,1)} %reshape.118), calls=%async_computation.3 | async-start | bytes 65536 | tf_op jit(solution)/shard_map/all_to_all | solution.py:37
  100.2 7.4 %all-to-all-start.4 = ((bf16[4,4,256]{2,0,1:T(4,128)(2,1)}), bf16[4,4,256]{2,0,1:T(4,128)(2,1)S(1)}, u32[]{:S(2)}, u32[]{:S(2)}) async-start(bf16[4,4,256]{2,0,1:T(4,128)(2,1)} %bitcast.11), calls=%async_computation.4 | async-start | bytes 16384 | tf_op jit(solution)/shard_map/all_to_all | solution.py:160
  103.5 117.8 %all-gather.5.cloned.1.call-start = ((), (), s32[]{:S(2)}) async-start(), calls=%async_computation.11 | async-start | bytes 1056768 | tf_op jit(solution)/shard_map/all_gather | solution.py:143
  108.0 136.1 %copy-start.6 = (bf16[32,1024]{1,0:T(8,128)(2,1)S(1)}, bf16[32,1024]{1,0:T(8,128)(2,1)}, u32[]{:S(2)}) copy-start(bf16[32,1024]{1,0:T(8,128)(2,1)} %param.33) | copy-start | bytes 196612
  143.5 3.4 collective-permute-start
  147.1 5.0 collective-permute-start.1
  173.1 22.2 %all-to-all-start.7 = ((bf16[128,2,256]{2,1,0:T(2,128)(2,1)}), bf16[128,2,256]{2,1,0:T(2,128)(2,1)S(1)}, u32[]{:S(2)}, u32[]{:S(2)}) async-start(bf16[128,2,256]{2,1,0:T(2,128)(2,1)} %copy.105), calls=%async_computation.7 | async-start | bytes 262144 | tf_op jit(solution)/shard_map/all_to_all | solution.py:183
  196.3 27.3 %all-to-all-start.8 = ((f32[4,4,256]{2,1,0:T(4,128)}), f32[4,4,256]{2,1,0:T(4,128)S(1)}, u32[]{:S(2)}, u32[]{:S(2)}) async-start(f32[4,4,256]{2,1,0:T(4,128)} %convolution_bitcast_fusion.1), calls=%async_computation.8 | async-start | bytes 32768 | tf_op jit(solution)/shard_map/all_to_all | solution.py:190
  248.4 8.6 %copy-start.9 = (bf16[1024]{0:T(1024)(128)(2,1)S(1)}, bf16[1024]{0:T(1024)(128)(2,1)}, u32[]{:S(2)}) copy-start(bf16[1024]{0:T(1024)(128)(2,1)} %param.34) | copy-start | bytes 6148
  248.4 8.6 %copy-start.3 = (bf16[1024,128]{1,0:T(8,128)(2,1)S(1)}, bf16[1024,128]{1,0:T(8,128)(2,1)}, u32[]{:S(2)}) copy-start(bf16[1024,128]{1,0:T(8,128)(2,1)} %param.24) | copy-start | bytes 786436
  248.4 9.3 %copy-start.4 = (bf16[1024,128]{1,0:T(8,128)(2,1)S(1)}, bf16[1024,128]{1,0:T(8,128)(2,1)}, u32[]{:S(2)}) copy-start(bf16[1024,128]{1,0:T(8,128)(2,1)} %param.25) | copy-start | bytes 786436
  248.4 264.0 %all-to-all-start.10 = ((bf16[128,32,1024]{2,1,0:T(8,128)(2,1)}), bf16[128,32,1024]{2,1,0:T(8,128)(2,1)}, u32[]{:S(2)}, u32[]{:S(2)}) async-start(bf16[128,32,1024]{2,1,0:T(8,128)(2,1)} %stack.2), calls=%async_computation.10 | async-start | bytes 16777216 | tf_op jit(solution)/shard_map/all_to_all | solution.py:148
Sparse Core Ops, SparseCore 0:
  150.3 70.9 all-gather.4
